TPU v7x, 256 devices: a whole 4x4x8 slice. The times are simulated.
256 devices in a mesh: sp: 32 (over z, x), tp: 8 (over y, core).
Axes of the slice: x: 4, y: 4, z: 8, core: 2. Of those that a mesh axis runs over, the one named last changes fastest.
Arguments:
- tokens: bfloat16 [24576, 4096], P('sp', 'tp'), may hold values from -6 to 6
- norm_gain: float32 [4096], replicated, may hold values from 0.1 to 1.9
- w_query: bfloat16 [4096, 2048], P('sp', 'tp'), may hold values from -0.09375 to 0.09375
- w_key: bfloat16 [4096, 1024], P('sp', 'tp'), may hold values from -0.09375 to 0.09375
- w_value: bfloat16 [4096, 1024], P('sp', 'tp'), may hold values from -0.09375 to 0.09375
- w_pool: bfloat16 [4096, 1024], P('sp', 'tp'), may hold values from -0.09375 to 0.09375
- query_gain: float32 [64], replicated, may hold values from 0.5 to 8
- key_gain: float32 [64], replicated, may hold values from 0.5 to 8
- sink_logit: float32 [32], P('tp'), may hold values from 1 to 5
- w_out_pool: bfloat16 [1024, 4096], P('tp', 'sp'), may hold values from -0.75 to 0.75
- w_out_attn: bfloat16 [2048, 4096], P('tp', 'sp'), may hold values from -1.5 to 1.5
Outputs:
- mixed: bfloat16 [24576, 4096], P(('sp', 'tp'))
All inputs are finite; a program needn't handle non-finite values.
Results may differ from a plain program's by a relative error of at most 0.014.
The roundings to bfloat16 on the way count: a program that leaves them out, or rounds other values in their place, can miss the bound.
Values may be sent and summed in bfloat16 or wider, within the bound.
No kernel may reach another device: no remote copies, remote signals or barrier semaphores. Data moves between devices by JAX's collectives and lax.ppermute only.
A program may use at most 128 MiB of HBM per device.

v0:
```python
import jax
import jax.numpy as jnp
from jax import lax
from jax.sharding import PartitionSpec as P

HEAD = 64
POOL = 1024
WINDOW = 128
GRID_W = 64
eps = 1e-06
rope_base = 10000.0
neg_big = -1e30
pool_reach = 8


def padded_2(block, sides, width):
    for axis, dim in sides:
        count = lax.axis_size(axis)
        forward = [(i, i + 1) for i in range(count - 1)]
        backward = [(target, source) for source, target in forward]
        low = lax.ppermute(
            lax.slice_in_dim(block, block.shape[dim] - width, None, axis=dim), axis, forward
        )
        high = lax.ppermute(lax.slice_in_dim(block, 0, width, axis=dim), axis, backward)
        block = jnp.concatenate([low, block, high], axis=dim)
    return block


def sent_together(arrays, axis, dim, along):
    ends, at = ([], 0)
    for a in arrays[:-1]:
        at += a.shape[along]
        ends.append(at)
    both = jnp.concatenate(arrays, axis=along)
    return tuple(jnp.split(lax.all_gather(both, axis, axis=dim, tiled=True), ends, axis=along))


def rope_tables(positions, head_size):
    quarter = head_size // 4
    freqs = 1.0 / rope_base ** (jnp.arange(quarter, dtype=jnp.float32) * 2.0 / (head_size // 2))
    row_angle = (positions // GRID_W).astype(jnp.float32)[:, None] * freqs
    col_angle = (positions % GRID_W).astype(jnp.float32)[:, None] * freqs
    angles = jnp.concatenate([row_angle, row_angle, col_angle, col_angle], axis=-1)
    return (jnp.cos(angles), jnp.sin(angles))


def rotate(heads_in, cosine, sine):
    part_one, part_two, part_three, part_four = jnp.split(heads_in, 4, axis=-1)
    turned = jnp.concatenate([-part_two, part_one, -part_four, part_three], axis=-1)
    return heads_in * cosine[:, None, :] + turned * sine[:, None, :]


def prepare(projected, gain, cosine, sine):
    rows_count = projected.shape[0]
    shaped = projected.reshape(rows_count, -1, HEAD)
    scaled = shaped * lax.rsqrt(jnp.mean(shaped * shaped, axis=-1, keepdims=True) + eps) * gain
    return rotate(scaled, cosine, sine).reshape(rows_count, -1).astype(jnp.bfloat16)


def edge_keys(keys_new, values_new):
    joined = jnp.concatenate([keys_new, values_new], axis=1)
    return padded_2(joined, (("sp", 0),), WINDOW)


def edge_pool(pool_in):
    return padded_2(pool_in, (("sp", 0),), pool_reach)


def window_attention(queries, key_band, sink_logit, positions, seq):
    rows_count = queries.shape[0]
    key_width = key_band.shape[1] // 2
    heads_q = queries.shape[1] // HEAD
    heads_k = key_width // HEAD
    group = heads_q // heads_k
    blocks = rows_count // WINDOW
    stacked = key_band.reshape(blocks + 2, WINDOW, 2 * key_width)
    joined = jnp.concatenate([stacked[:-2], stacked[1:-1], stacked[2:]], axis=1)
    block_keys = joined[:, :, :key_width].reshape(blocks, 3 * WINDOW, heads_k, HEAD)
    block_values = joined[:, :, key_width:].reshape(blocks, 3 * WINDOW, heads_k, HEAD)
    block_queries = queries.reshape(blocks, WINDOW, heads_k, group, HEAD)
    scores = jnp.einsum(
        "nqhgd,nkhd->nhgqk", block_queries, block_keys, preferred_element_type=jnp.float32
    ) * HEAD ** (-0.5)
    query_pos = positions.reshape(blocks, WINDOW)
    key_pos = query_pos[:, :1] - WINDOW + jnp.arange(3 * WINDOW, dtype=jnp.int32)[None, :]
    inside = (
        (jnp.abs(query_pos[:, :, None] - key_pos[:, None, :]) <= WINDOW)
        & (key_pos[:, None, :] >= 0)
        & (key_pos[:, None, :] < seq)
    )
    scores = jnp.where(inside[:, None, None], scores, neg_big)
    sink = sink_logit.reshape(heads_k, group)[None, :, :, None, None]
    top = jnp.maximum(jnp.max(scores, axis=-1, keepdims=True), sink)
    raised = jnp.exp(scores - top)
    totals = jnp.sum(raised, axis=-1, keepdims=True) + jnp.exp(sink - top)
    weights = (raised / totals).astype(jnp.bfloat16)
    result = jnp.einsum(
        "nhgqk,nkhd->nqhgd", weights, block_values, preferred_element_type=jnp.float32
    )
    return result.astype(jnp.bfloat16).reshape(rows_count, heads_q * HEAD)


def window_pool(pool_band, pool_in, positions, seq):
    rows_count = pool_in.shape[0]
    level = lax.axis_index("tp") * pool_in.shape[1] // (POOL // 4)
    padded = pool_band.astype(jnp.float32)
    sum_two = padded[:-1] + padded[1:]
    sum_four = sum_two[:-2] + sum_two[2:]
    sum_eight = sum_four[:-4] + sum_four[4:]
    sum_sixteen = sum_eight[:-8] + sum_eight[8:]
    candidates = jnp.stack(
        [
            sum_two[7 : 7 + rows_count],
            sum_four[6 : 6 + rows_count],
            sum_eight[4 : 4 + rows_count],
            sum_sixteen[:rows_count],
        ]
    )
    chosen = lax.dynamic_index_in_dim(candidates, level, 0, keepdims=False)
    reach = jnp.left_shift(jnp.int32(1), level)
    low = jnp.clip(positions - reach, 0, seq - 1)
    high = jnp.clip(positions + reach - 1, 0, seq - 1)
    counted = (high - low + 1).astype(jnp.float32)
    return (chosen / counted[:, None]).astype(jnp.bfloat16)


def shards(
    tokens,
    norm_gain,
    w_query,
    w_key,
    w_value,
    w_pool,
    query_gain,
    key_gain,
    sink_logit,
    w_out_pool,
    w_out_attn,
):
    gathered = lax.all_gather(tokens, "tp", axis=1, tiled=True)
    rows_count = gathered.shape[0]
    widened = gathered.astype(jnp.float32)
    normed = (
        widened * lax.rsqrt(jnp.mean(widened * widened, axis=1, keepdims=True) + eps) * norm_gain
    ).astype(jnp.bfloat16)
    positions = lax.axis_index("sp") * rows_count + jnp.arange(rows_count, dtype=jnp.int32)
    seq = lax.axis_size("sp") * rows_count
    cosine, sine = rope_tables(positions, HEAD)
    pieces = sent_together((w_query, w_key, w_value, w_pool), "sp", 0, 1)
    query_raw, key_raw, value_raw, pool_raw = tuple(
        (jnp.dot(normed, piece, preferred_element_type=jnp.float32) for piece in pieces)
    )
    queries = prepare(query_raw, query_gain, cosine, sine)
    keys_new = prepare(key_raw, key_gain, cosine, sine)
    pool_in = pool_raw.astype(jnp.bfloat16)
    key_band = edge_keys(keys_new, value_raw.astype(jnp.bfloat16))
    pool_band = edge_pool(pool_in)
    pooled = window_pool(pool_band, pool_in, positions, seq)
    attended = window_attention(queries, key_band, sink_logit, positions, seq)
    out_pool, out_attn = sent_together((w_out_pool, w_out_attn), "sp", 1, 0)
    return lax.psum_scatter(
        (
            jnp.dot(pooled, out_pool, preferred_element_type=jnp.float32)
            + jnp.dot(attended, out_attn, preferred_element_type=jnp.float32)
        ).astype(jnp.bfloat16),
        "tp",
        scatter_dimension=0,
        tiled=True,
    )


def solution(mesh):
    placed = (
        P("sp", "tp"),
        P(),
        P("sp", "tp"),
        P("sp", "tp"),
        P("sp", "tp"),
        P("sp", "tp"),
        P(),
        P(),
        P("tp"),
        P("tp", "sp"),
        P("tp", "sp"),
    )
    return jax.shard_map(
        shards, mesh=mesh, in_specs=placed, out_specs=P(("sp", "tp"), None), check_vma=False
    )
```

profile of v0, /device:TPU:1, one launch (start us, length us, event | category | flops | bytes accessed | tf_op | source)
XLA Modules:
  0.0 294.5 jit_solution(10621798535016886993)
XLA Ops:
  6.5 0.7 all-gather.4.cloned.1.call-update
  7.3 1.6 pad_maximum_fusion.7
  9.0 1.5 pad_maximum_fusion.8
  10.6 0.1 add_reduce_fusion
  10.9 0.7 max.27
  11.6 0.7 mul.195
  12.3 0.1 mul.196
  12.3 0.7 mul.217
  13.2 0.4 fusion.37
  13.5 1.4 fusion.12
  14.9 41.9 %all-gather.4.cloned.1.call-done = bf16[768,4096]{1,0:T(8,128)(2,1)} async-done(((bf16[768,512]{1,0:T(8,128)(2,1)}), bf16[768,4096]{1,0:T(8,128)(2,1)}) %all-gather.4.cloned.1.call-update) | async-done | bytes 6291472 | tf_op jit(solution)/shard_map/all_gather | solution.py:140
  56.8 4.2 %fusion = f32[768]{0:T(1024)S(1)} fusion(bf16[768,4096]{1,0:T(8,128)(2,1)} %all-gather.4.cloned.1.call-done), kind=kLoop, calls=%fused_computation.2 | loop fusion | flops 9436416 | bytes 6294528 | tf_op jit(solution)/shard_map/reduce_sum | solution.py:144
  61.1 0.4 copy-done.1
  61.4 5.4 %fusion.2 = bf16[768,4096]{1,0:T(8,128)(2,1)} fusion(bf16[768,4096]{1,0:T(8,128)(2,1)S(1)} %copy-done.1, f32[4096]{0:T(1024)S(1)} %copy-done.3, f32[768]{0:T(1024)S(1)} %add_rsqrt_fusion.2), kind=kLoop, calls=%fused_computation.4 | loop fusion | flops 12582912 | bytes 12602368 | tf_op jit(solution)/shard_map/convert_element_type | solution.py:145
  66.8 74.1 %all-gather.6.cloned.1.call-done = bf16[4096,640]{1,0:T(8,128)(2,1)} async-done(((bf16[128,640]{1,0:T(8,128)(2,1)}), bf16[4096,640]{1,0:T(8,128)(2,1)}) %all-gather.6.cloned.1.call-update) | async-done | bytes 5242896 | tf_op jit(solution)/shard_map/all_gather | solution.py:35
  140.8 5.0 %convolution_convert_fusion.1 = bf16[768,128]{1,0:T(8,128)(2,1)S(1)} fusion(bf16[768,4096]{1,0:T(8,128)(2,1)} %fusion.2, bf16[4096,640]{1,0:T(8,128)(2,1)} %all-gather.6.cloned.1.call-done), kind=kOutput, calls=%fused_computation.26 | convolution fusion | flops 805404672 | bytes 7536640 | tf_op jit(solution)/shard_map/dot_general | solution.py:151
  145.8 1.9 collective-permute-start
  147.7 1.6 collective-permute-start.1
  149.3 3.5 %multiply_reduce_fusion.1 = (f32[768,2]{0,1:T(2,128)S(1)}, f32[768,128]{0,1:T(8,128)S(1)}) fusion(bf16[768,4096]{1,0:T(8,128)(2,1)S(1)} %copy-done, bf16[4096,640]{1,0:T(8,128)(2,1)} %all-gather.6.cloned.1.call-done), kind=kOutput, calls=%fused_computation.74 | convolution fusion | flops 805501440 | bytes 7739392 | tf_op jit(solution)/shard_map/dot_general | solution.py:151
  152.8 0.1 multiply_multiply_fusion.1
  153.0 0.1 fusion.29
  153.2 2.2 convolution_convert_fusion
  155.4 4.0 %collective-permute-start.2 = (bf16[128,256]{0,1:T(8,128)(2,1)S(1)}, bf16[128,256]{0,1:T(8,128)(2,1)S(1)}, u32[]{:S(2)}, u32[]{:S(2)}) collective-permute-start(bf16[128,256]{0,1:T(8,128)(2,1)S(1)} %get-tuple-element.16), channel_id=1, source_target_pairs={{0,8},{8,16},{16,24},{24,32},{32,40},{40,48},{48,56},{56,64},{64,7... | collective-permute-start | bytes 196616 | tf_op jit(solution)/shard_map/ppermute | solution.py:21
  159.4 1.5 collective-permute-start.3
  160.9 2.0 multiply_reduce_fusion
  162.9 0.1 multiply_multiply_fusion
  163.2 0.2 fusion.19
  163.4 0.5 reshape.301
  164.3 54.8 %all-gather.8.cloned.1.call-done = bf16[384,4096]{1,0:T(8,128)(2,1)} async-done(((bf16[384,128]{1,0:T(8,128)(2,1)}), bf16[384,4096]{1,0:T(8,128)(2,1)}) %all-gather.8.cloned.1.call-update) | async-done | bytes 3145744 | tf_op jit(solution)/shard_map/all_gather | solution.py:35
  219.1 7.6 %fusion.16 = f32[768,4096]{1,0:T(8,128)} fusion(bf16[384,4096]{1,0:T(8,128)(2,1)} %all-gather.8.cloned.1.call-done, s32[]{:T(128)S(6)} %select_n.33, f32[1,768,128]{2,1,0:T(8,128)S(1)} %get-tuple-element.38, f32[1,768,128]{2,1,0:T(8,128)S(1)} %get-tuple-element.39, f32[1,768,128]{2,1,0:T(8,128)S(1)} %get-tuple-element.40, ...), kind=kOutput, calls=%fused_computation.30 | convolution fusion | flops 805797888 | bytes 15207428 | tf_op jit(solution)/shard_map/dot_general | solution.py:163
  226.7 0.1 pad_maximum_fusion.4
  226.8 0.2 copy.34
  226.9 0.2 copy.36
  227.1 0.2 copy.35
  227.4 0.3 fusion.53
  227.6 0.3 copy.38
  228.0 0.3 copy.37
  228.3 1.0 fusion.4
  229.3 1.0 fusion.3
  230.4 0.1 exponential_add_fusion
  230.5 1.4 fusion.10
  231.8 0.3 copy.41
  232.1 0.5 slice-done
  232.6 1.3 slice-done.1
  233.9 1.2 slice-done.2
  235.1 0.9 copy-done.2
  236.0 4.5 %add_convert_fusion = bf16[768,4096]{1,0:T(8,128)(2,1)} fusion(f32[768,4096]{1,0:T(8,128)S(1)} %bitcast.93, bf16[384,4096]{1,0:T(8,128)(2,1)S(1)} %copy-done.2, bf16[32,8,6,128]{3,2,1,0:T(8,128)(2,1)S(1)} %bitcast.95), kind=kOutput, calls=%fused_computation.5 | convolution fusion | flops 1616904192 | bytes 21495808 | tf_op jit(solution)/shard_map/dot_general | solution.py:164
  240.6 47.4 %reduce-scatter.2.cloned.1.call-done = bf16[96,4096]{1,0:T(8,128)(2,1)} async-done(((bf16[768,4096]{1,0:T(8,128)(2,1)}), bf16[96,4096]{1,0:T(8,128)(2,1)}) %reduce-scatter.2.cloned.1.call-update) | async-done | bytes 786448 | tf_op jit(solution)/shard_map/reduce_scatter | solution.py:161
  (56 shorter events, 1.3 us)
Async XLA Ops:
  6.5 54.5 %copy-start.3 = (f32[4096]{0:T(1024)S(1)}, f32[4096]{0:T(1024)}, u32[]{:S(2)}) copy-start(f32[4096]{0:T(1024)} %param.12) | copy-start | bytes 49156
  6.5 50.3 %all-gather.4.cloned.1.call-start = ((), (), s32[]{:S(2)}) async-start(), calls=%async_computation.1 | async-start | bytes 7077888 | tf_op jit(solution)/shard_map/all_gather | solution.py:140
  7.3 133.6 %all-gather.6.cloned.1.call-start = ((), (), s32[]{:S(2)}) async-start(), calls=%async_computation.2 | async-start | bytes 5406720 | tf_op jit(solution)/shard_map/all_gather | solution.py:35
  8.9 210.1 %all-gather.8.cloned.1.call-start = ((), (), s32[]{:S(2)}) async-start(), calls=%async_computation.3 | async-start | bytes 3244032 | tf_op jit(solution)/shard_map/all_gather | solution.py:35
  10.5 277.5 %reduce-scatter.2.cloned.1.call-start = ((), (), s32[]{:S(2)}) async-start(), calls=%async_computation.4 | async-start | bytes 7077888 | tf_op jit(solution)/shard_map/reduce_scatter | solution.py:161
  56.8 4.6 %copy-start.1 = (bf16[768,4096]{1,0:T(8,128)(2,1)S(1)}, bf16[768,4096]{1,0:T(8,128)(2,1)}, u32[]{:S(2)}) copy-start(bf16[768,4096]{1,0:T(8,128)(2,1)} %all-gather.4.cloned.1.call-done) | copy-start | bytes 18874372
  140.8 8.5 %copy-start = (bf16[768,4096]{1,0:T(8,128)(2,1)S(1)}, bf16[768,4096]{1,0:T(8,128)(2,1)}, u32[]{:S(2)}) copy-start(bf16[768,4096]{1,0:T(8,128)(2,1)} %fusion.2) | copy-start | bytes 18874372
  145.8 18.1 %collective-permute-start = (bf16[8,128]{1,0:T(8,128)(2,1)S(1)}, bf16[8,128]{1,0:T(8,128)(2,1)S(1)}, u32[]{:S(2)}, u32[]{:S(2)}) collective-permute-start(bf16[8,128]{1,0:T(8,128)(2,1)S(1)} %get-tuple-element.22), channel_id=1, source_target_pairs={{0,8},{8,16},{16,24},{24,32},{32,40},{40,48},{48,56},{56,64},{64,7... | collective-permute-start | bytes 6152 | tf_op jit(solution)/shard_map/ppermute | solution.py:21
  147.7 5.4 %slice-start.3 = ((s8[5242880]{0:T(1024)(128)(4,1)}), s8[4194304]{0:T(1024)(128)(4,1)S(1)}, s32[]{:S(2)}) async-start(s8[5242880]{0:T(1024)(128)(4,1)} %bitcast.99), calls=%async_computation.8 | async-start | bytes 8388608
  147.7 5.1 %copy-start.5 = (f32[64]{0:T(128)S(1)}, f32[64]{0:T(128)}, u32[]{:S(2)}) copy-start(f32[64]{0:T(128)} %param.18) | copy-start | bytes 772
  147.7 5.4 %slice-start.4 = ((s8[5242880]{0:T(1024)(128)(4,1)}), s8[1048576]{0:T(1024)(128)(4,1)S(1)}, s32[]{:S(2)}) async-start(s8[5242880]{0:T(1024)(128)(4,1)} %bitcast.99), calls=%async_computation.9 | async-start | bytes 2097152
  147.7 16.2 %collective-permute-start.1 = (bf16[8,128]{1,0:T(8,128)(2,1)S(1)}, bf16[8,128]{1,0:T(8,128)(2,1)S(1)}, u32[]{:S(2)}, u32[]{:S(2)}) collective-permute-start(bf16[8,128]{1,0:T(8,128)(2,1)S(1)} %get-tuple-element.23), channel_id=1, source_target_pairs={{8,0},{16,8},{24,16},{32,24},{40,32},{48,40},{56,48},{64,56},{72,6... | collective-permute-start | bytes 6152 | tf_op jit(solution)/shard_map/ppermute | solution.py:24
  155.4 71.3 %collective-permute-start.2 = (bf16[128,256]{0,1:T(8,128)(2,1)S(1)}, bf16[128,256]{0,1:T(8,128)(2,1)S(1)}, u32[]{:S(2)}, u32[]{:S(2)}) collective-permute-start(bf16[128,256]{0,1:T(8,128)(2,1)S(1)} %get-tuple-element.16), channel_id=1, source_target_pairs={{0,8},{8,16},{16,24},{24,32},{32,40},{40,48},{48,56},{56,64},{64,7... | collective-permute-start | bytes 196616 | tf_op jit(solution)/shard_map/ppermute | solution.py:21
  159.4 3.5 %copy-start.4 = (f32[64]{0:T(128)S(1)}, f32[64]{0:T(128)}, u32[]{:S(2)}) copy-start(f32[64]{0:T(128)} %param.17) | copy-start | bytes 772
  159.4 67.2 %collective-permute-start.3 = (bf16[128,256]{0,1:T(8,128)(2,1)S(1)}, bf16[128,256]{0,1:T(8,128)(2,1)S(1)}, u32[]{:S(2)}, u32[]{:S(2)}) collective-permute-start(bf16[128,256]{0,1:T(8,128)(2,1)S(1)} %get-tuple-element.17), channel_id=1, source_target_pairs={{8,0},{16,8},{24,16},{32,24},{40,32},{48,40},{56,48},{64,56},{72,6... | collective-permute-start | bytes 196616 | tf_op jit(solution)/shard_map/ppermute | solution.py:24
  230.4 2.2 slice-start
  230.5 3.5 %slice-start.1 = ((s8[12582912]{0:T(1024)(128)(4,1)}), s8[4194304]{0:T(1024)(128)(4,1)S(1)}, s32[]{:S(2)}) async-start(s8[12582912]{0:T(1024)(128)(4,1)} %bitcast.92), calls=%async_computation.6 | async-start | bytes 8388608
  230.5 4.6 %slice-start.2 = ((s8[12582912]{0:T(1024)(128)(4,1)}), s8[4194304]{0:T(1024)(128)(4,1)S(1)}, s32[]{:S(2)}) async-start(s8[12582912]{0:T(1024)(128)(4,1)} %bitcast.92), calls=%async_computation.7 | async-start | bytes 8388608
  230.5 5.5 %copy-start.2 = (bf16[384,4096]{1,0:T(8,128)(2,1)S(1)}, bf16[384,4096]{1,0:T(8,128)(2,1)}, u32[]{:S(2)}) copy-start(bf16[384,4096]{1,0:T(8,128)(2,1)} %all-gather.8.cloned.1.call-done) | copy-start | bytes 9437188
Sparse Core Ops, SparseCore 0:
  9.2 47.6 all-gather.3
  59.4 81.3 all-gather.5
  143.3 75.7 all-gather.7
  240.7 47.2 reduce-scatter.1
where the time goes:
time: 295 us
  waiting for transfers between devices  219 us (74%)
  matrix products  27.1 us (9%)
  other arithmetic  17.2 us (6%)
  between operations  13.6 us (5%)
  starting transfers between devices  9 us (3%)
  local copies, waits for them, and re-layouts  8.74 us (3%)
    all_gather x2, waiting for transfers between devices, sent_together(): lax.all_gather(both, axis, axis=dim, tiled=True)  129 us
    reduce_scatter x1, waiting for transfers between devices, shards(): lax.psum_scatter((jnp.dot(pooled, out_pool, preferred_element_type=jnp.fl...  47.4 us
    all_gather x1, waiting for transfers between devices, shards(): gathered = lax.all_gather(tokens, 'tp', axis=1, tiled=True)  41.9 us
    dot_general x4, matrix products, shards(): jnp.dot(normed, piece, preferred_element_type=jnp.float32)  12.7 us
    dot_general x1, matrix products, shards(): jnp.dot(pooled, out_pool, preferred_element_type=jnp.float32)  7.6 us
  transfers between devices with their start and end apart: 8, of which 4 were waited for; matrix products, arithmetic and copies ran while one was open for 13% of the time, Pallas kernels for 0%

commit v1 on v0

--- a/solution.py
+++ b/solution.py
@@ -11,6 +11,28 @@
 rope_base = 10000.0
 neg_big = -1e30
 pool_reach = 8
+
+
+def in_order(blocks, dim):
+    lengths = list(blocks.shape[1:])
+    lengths[dim] *= blocks.shape[0]
+    return jnp.moveaxis(blocks, 0, dim).reshape(lengths)
+
+
+def gather_around(value, axis, dim):
+    devices = lax.axis_size(axis)
+    pairs = [(i, (i + 1) % devices) for i in range(devices)]
+    back = [(b, a) for a, b in pairs]
+    lower, upper = ([], [])
+    for step in range(devices - 1):
+        if step % 2 == 0:
+            lower.append(lax.ppermute(lower[-1] if lower else value, axis, pairs))
+        else:
+            upper.append(lax.ppermute(upper[-1] if upper else value, axis, back))
+    tiles = jnp.stack([*lower[::-1], value, *upper])
+    shift = lax.axis_index(axis) - len(lower)
+    tiles = tiles[(jnp.arange(devices) - shift) % devices]
+    return in_order(tiles, dim)
 
 
 def padded_2(block, sides, width):
@@ -137,7 +159,7 @@
     w_out_pool,
     w_out_attn,
 ):
-    gathered = lax.all_gather(tokens, "tp", axis=1, tiled=True)
+    gathered = gather_around(tokens, "tp", 1)
     rows_count = gathered.shape[0]
     widened = gathered.astype(jnp.float32)
     normed = (

time: 295 us -> 254 us (0.86)
  waiting for transfers between devices: 219 us -> 96.2 us
  local copies, waits for them, and re-layouts: 8.74 us -> 52.6 us
  starting transfers between devices: 9 us -> 29.9 us
  other arithmetic: 17.2 us -> 34 us
    all_gather x2, waiting for transfers between devices: 129 us -> 27.3 us  [sent_together(): lax.all_gather(both, axis, axis=dim, tiled=True)]
    all_gather x1 -> x0, waiting for transfers between devices: 41.9 us -> none  [shards(): gathered = lax.all_gather(tokens, 'tp', axis=1, tiled=True)]
    ppermute x0 -> x7, waiting for transfers between devices: none -> 21.4 us  [the longest x4 21.2 us: gather_around(): lower.append(lax.ppermute(lower[-1] if lower else value, axis, pairs))]
    ppermute x0 -> x7, starting transfers between devices: none -> 18.7 us  [the longest x4 10 us: gather_around(): lower.append(lax.ppermute(lower[-1] if lower else value, axis, pairs))]
    convert_element_type x0 -> x2, local copies, waits for them, and re-layouts: none -> 13.1 us  [the longest x1 12.7 us: shards(): widened = gathered.astype(jnp.float32)]
    unnamed x22 -> x51, local copies, waits for them, and re-layouts: 4.27 us -> 12.3 us
    mul x4 -> x2, local copies, waits for them, and re-layouts: 1.48 us -> 9.38 us  [shards(): widened * lax.rsqrt(jnp.mean(widened * widened, axis=1, keepdims=True) +...]
    dot_general x0 -> x4, local copies, waits for them, and re-layouts: none -> 7.62 us  [shards(): jnp.dot(normed, piece, preferred_element_type=jnp.float32)]
  transfers between devices with their start and end apart: 8 -> 14, of which waited for: 4 -> 7; matrix products, arithmetic and copies ran while one was open for 13% -> 37% of each run, Pallas kernels for 0% -> 0%
where the time goes in v1:
time: 254 us
  waiting for transfers between devices  96.2 us (38%)
  local copies, waits for them, and re-layouts  52.6 us (21%)
  other arithmetic  34 us (13%)
  starting transfers between devices  29.9 us (12%)
  matrix products  27.2 us (11%)
  between operations  13.6 us (5%)
    reduce_scatter x1, waiting for transfers between devices, shards(): lax.psum_scatter((jnp.dot(pooled, out_pool, preferred_element_type=jnp.fl...  47.5 us
    all_gather x2, waiting for transfers between devices, sent_together(): lax.all_gather(both, axis, axis=dim, tiled=True)  27.3 us
    ppermute x4, waiting for transfers between devices, gather_around(): lower.append(lax.ppermute(lower[-1] if lower else value, axis, pairs))  21.2 us
    convert_element_type x1, local copies, waits for them, and re-layouts, shards(): widened = gathered.astype(jnp.float32)  12.7 us
    unnamed x51, local copies, waits for them, and re-layouts  12.3 us
    dot_general x4, matrix products, shards(): jnp.dot(normed, piece, preferred_element_type=jnp.float32)  10.2 us
    ppermute x4, starting transfers between devices, gather_around(): lower.append(lax.ppermute(lower[-1] if lower else value, axis, pairs))  10 us
    mul x2, local copies, waits for them, and re-layouts, shards(): widened * lax.rsqrt(jnp.mean(widened * widened, axis=1, keepdims=True) +...  9.38 us
  transfers between devices with their start and end apart: 14, of which 7 were waited for; matrix products, arithmetic and copies ran while one was open for 37% of the time, Pallas kernels for 0%

profile of v1, /device:TPU:1, one launch (start us, length us, event | category | flops | bytes accessed | tf_op | source)
XLA Modules:
  0.0 253.6 jit_solution(12001963821651043041)
XLA Ops:
  6.5 1.6 pad_maximum_fusion.7
  8.3 2.7 %collective-permute-start = (bf16[768,512]{1,0:T(8,128)(2,1)}, bf16[768,512]{1,0:T(8,128)(2,1)S(1)}, u32[]{:S(2)}, u32[]{:S(2)}) collective-permute-start(bf16[768,512]{1,0:T(8,128)(2,1)} %param.11), channel_id=1, source_target_pairs={{0,1},{1,2},{2,3},{3,4},{4,5},{5,6},{6,7},{7,0},{8,9},{9,10},{10,1... | collective-permute-start | bytes 2359304 | tf_op jit(solution)/shard_map/ppermute | solution.py:29
  10.9 9.3 %collective-permute-done = bf16[768,512]{1,0:T(8,128)(2,1)S(1)} collective-permute-done((bf16[768,512]{1,0:T(8,128)(2,1)}, bf16[768,512]{1,0:T(8,128)(2,1)S(1)}, u32[]{:S(2)}, u32[]{:S(2)}) %collective-permute-start) | collective-permute-done | bytes 786464 | tf_op jit(solution)/shard_map/ppermute | solution.py:29
  20.2 2.4 collective-permute-start.1
  22.6 1.7 collective-permute-start.4
  24.3 1.5 pad_maximum_fusion.8
  27.4 4.1 %collective-permute-done.1 = bf16[768,512]{1,0:T(8,128)(2,1)S(1)} collective-permute-done((bf16[768,512]{1,0:T(8,128)(2,1)S(1)}, bf16[768,512]{1,0:T(8,128)(2,1)S(1)}, u32[]{:S(2)}, u32[]{:S(2)}) %collective-permute-start.1) | collective-permute-done | bytes 786464 | tf_op jit(solution)/shard_map/ppermute | solution.py:29
  31.5 2.5 collective-permute-start.2
  34.2 1.1 fusion.36
  35.3 3.0 %collective-permute-start.5 = (bf16[768,512]{1,0:T(8,128)(2,1)S(1)}, bf16[768,512]{1,0:T(8,128)(2,1)S(1)}, u32[]{:S(2)}, u32[]{:S(2)}) collective-permute-start(bf16[768,512]{1,0:T(8,128)(2,1)S(1)} %collective-permute-done.4), channel_id=1, source_target_pairs={{1,0},{2,1},{3,2},{4,3},{5,4},{6,5},{7,6},{0,7},{9,8},{10,9},{11,1... | collective-permute-start | bytes 2359304 | tf_op jit(solution)/shard_map/ppermute | solution.py:31
  38.3 4.6 %collective-permute-done.2 = bf16[768,512]{1,0:T(8,128)(2,1)S(1)} collective-permute-done((bf16[768,512]{1,0:T(8,128)(2,1)S(1)}, bf16[768,512]{1,0:T(8,128)(2,1)S(1)}, u32[]{:S(2)}, u32[]{:S(2)}) %collective-permute-start.2) | collective-permute-done | bytes 786464 | tf_op jit(solution)/shard_map/ppermute | solution.py:29
  42.9 2.5 collective-permute-start.3
  45.6 1.4 fusion.13
  47.2 4.0 %collective-permute-start.6 = (bf16[768,512]{1,0:T(8,128)(2,1)S(1)}, bf16[768,512]{1,0:T(8,128)(2,1)S(1)}, u32[]{:S(2)}, u32[]{:S(2)}) collective-permute-start(bf16[768,512]{1,0:T(8,128)(2,1)S(1)} %collective-permute-done.5), channel_id=1, source_target_pairs={{1,0},{2,1},{3,2},{4,3},{5,4},{6,5},{7,6},{0,7},{9,8},{10,9},{11,1... | collective-permute-start | bytes 2359304 | tf_op jit(solution)/shard_map/ppermute | solution.py:31
  51.1 3.2 %collective-permute-done.3 = bf16[768,512]{1,0:T(8,128)(2,1)S(1)} collective-permute-done((bf16[768,512]{1,0:T(8,128)(2,1)S(1)}, bf16[768,512]{1,0:T(8,128)(2,1)S(1)}, u32[]{:S(2)}, u32[]{:S(2)}) %collective-permute-start.3) | collective-permute-done | bytes 786464 | tf_op jit(solution)/shard_map/ppermute | solution.py:29
  54.3 1.0 bitcast_dynamic-update-slice_fusion.7
  55.3 0.9 bitcast_dynamic-update-slice_fusion.6
  57.2 1.0 bitcast_dynamic-update-slice_fusion.4
  60.0 1.0 bitcast_dynamic-update-slice_fusion.1
  61.9 6.7 %gather_fusion = bf16[8,768,512]{2,1,0:T(8,128)(2,1)} fusion(bf16[8,768,512]{2,1,0:T(8,128)(2,1)} %bitcast_dynamic-update-slice_fusion, s32[1024]{0:T(1024)S(1)} %pad_clamp_fusion), kind=kCustom, calls=%fused_computation | custom fusion | bytes 12582944 | tf_op jit(solution)/shard_map/gather | solution.py:34
  68.6 4.3 %fusion = f32[768]{0:T(1024)S(1)} fusion(bf16[8,768,512]{2,1,0:T(8,128)(2,1)} %gather_fusion), kind=kLoop, calls=%fused_computation.4 | loop fusion | flops 9436416 | bytes 6294528 | tf_op jit(solution)/shard_map/reduce_sum | solution.py:166
  73.4 6.3 %convert_bitcast_fusion = f32[768,8,512]{2,0,1:T(8,128)} fusion(bf16[8,768,512]{2,1,0:T(8,128)(2,1)S(1)} %copy-done), kind=kLoop, calls=%fused_computation.3 | loop fusion | flops 3145728 | bytes 18874368 | tf_op jit(solution)/shard_map/convert_element_type | solution.py:164
  79.8 4.6 %fusion.5 = bf16[768,8,512]{2,0,1:T(8,128)(2,1)} fusion(bf16[8,768,512]{2,1,0:T(8,128)(2,1)S(1)} %copy-done, f32[8,512]{1,0:T(8,128)S(1)} %mul.171, f32[768]{0:T(1024)S(1)} %add_rsqrt_fusion.2), kind=kLoop, calls=%fused_computation.11 | loop fusion | flops 12582912 | bytes 12602368 | tf_op jit(solution)/shard_map/mul | solution.py:166
  84.4 8.7 %copy.62 = bf16[768,8,512]{0,2,1:T(8,128)(2,1)} copy(bf16[768,8,512]{2,0,1:T(8,128)(2,1)} %fusion.5) | data formatting | bytes 12582912 | tf_op jit(solution)/shard_map/mul | solution.py:166
  93.0 12.7 %copy.61 = f32[768,8,512]{0,2,1:T(8,128)} copy(f32[768,8,512]{2,0,1:T(8,128)} %convert_bitcast_fusion) | data formatting | bytes 25165824 | tf_op jit(solution)/shard_map/convert_element_type | solution.py:164
  105.7 8.7 %fusion.4 = bf16[768,4096]{0,1:T(8,128)(2,1)} fusion(f32[768,8,512]{0,2,1:T(8,128)} %copy.61, f32[4096]{0:T(1024)S(1)} %copy-done.12, f32[768]{0:T(1024)S(1)} %add_rsqrt_fusion.2), kind=kLoop, calls=%fused_computation.9 | loop fusion | flops 9437184 | bytes 18893824 | tf_op jit(solution)/shard_map/convert_element_type | solution.py:167
  114.4 1.7 slice_bitcast_fusion
  116.2 3.1 %copy.70 = bf16[256,4096]{1,0:T(8,128)(2,1)} copy(bf16[256,4096]{0,1:T(8,128)(2,1)S(1)} %slice_bitcast_fusion) | data formatting | bytes 4194304 | tf_op jit(solution)/shard_map/dot_general | solution.py:173
  119.2 1.5 slice_bitcast_fusion.1
  120.7 1.3 copy.63
  122.0 5.0 %convolution_convert_fusion.1 = bf16[768,128]{1,0:T(8,128)(2,1)S(1)} fusion(bf16[768,4096]{0,1:T(8,128)(2,1)} %fusion.4, bf16[4096,640]{1,0:T(8,128)(2,1)} %all-gather.3.cloned.1.call-done), kind=kOutput, calls=%fused_computation.31 | convolution fusion | flops 805404672 | bytes 7536640 | tf_op jit(solution)/shard_map/dot_general | solution.py:173
  127.1 3.1 %collective-permute-start.7 = (bf16[8,128]{1,0:T(8,128)(2,1)S(1)}, bf16[8,128]{1,0:T(8,128)(2,1)S(1)}, u32[]{:S(2)}, u32[]{:S(2)}) collective-permute-start(bf16[8,128]{1,0:T(8,128)(2,1)S(1)} %get-tuple-element.22), channel_id=1, source_target_pairs={{0,8},{8,16},{16,24},{24,32},{32,40},{40,48},{48,56},{56,64},{64,7... | collective-permute-start | bytes 6152 | tf_op jit(solution)/shard_map/ppermute | solution.py:43
  130.2 1.5 collective-permute-start.8
  131.8 1.0 multiply_reduce_fusion.1
  132.9 1.8 multiply_reduce_fusion
  135.9 2.3 convolution_convert_fusion
  139.4 1.3 collective-permute-start.10
  140.7 5.2 %collective-permute-start.9 = (bf16[128,256]{0,1:T(8,128)(2,1)S(1)}, bf16[128,256]{0,1:T(8,128)(2,1)}, u32[]{:S(2)}, u32[]{:S(2)}) collective-permute-start(bf16[128,256]{0,1:T(8,128)(2,1)S(1)} %get-tuple-element.16), channel_id=1, source_target_pairs={{0,8},{8,16},{16,24},{24,32},{32,40},{40,48},{48,56},{56,64},{64,7... | collective-permute-start | bytes 196616 | tf_op jit(solution)/shard_map/ppermute | solution.py:43
  146.3 27.3 %all-gather.5.cloned.1.call-done = bf16[384,4096]{1,0:T(8,128)(2,1)} async-done(((bf16[384,128]{1,0:T(8,128)(2,1)}), bf16[384,4096]{1,0:T(8,128)(2,1)}) %all-gather.5.cloned.1.call-update) | async-done | bytes 3145744 | tf_op jit(solution)/shard_map/all_gather | solution.py:57
  173.6 7.6 %fusion.15 = f32[768,4096]{1,0:T(8,128)} fusion(bf16[384,4096]{1,0:T(8,128)(2,1)} %all-gather.5.cloned.1.call-done, s32[]{:T(128)S(6)} %select_n.58, f32[1,768,128]{2,1,0:T(8,128)S(1)} %get-tuple-element.38, f32[1,768,128]{2,1,0:T(8,128)S(1)} %get-tuple-element.39, f32[1,768,128]{2,1,0:T(8,128)S(1)} %get-tuple-element.40, ...), kind=kOutput, calls=%fused_computation.34 | convolution fusion | flops 805797888 | bytes 15207428 | tf_op jit(solution)/shard_map/dot_general | solution.py:185
  181.3 1.0 pad_maximum_fusion.4
  183.4 1.0 fusion.7
  184.5 2.0 copy-done.1
  186.5 1.1 fusion.6
  188.0 3.8 %fusion.11 = bf16[6,128,2,2,64]{1,4,3,2,0:T(8,128)(2,1)S(1)} fusion(bf16[6,384,2,64,1]{1,3,4,2,0:T(8,128)(2,1)S(1)} %bitcast.116, f32[6,2,384,128,2]{3,2,4,1,0:T(8,128)} %copy-done.1, f32[6,2,2,128]{3,2,1,0:T(2,128)S(1)} %exponential_add_fusion, f32[6,2,2,128]{3,2,1,0:T(2,128)S(1)} %broadcast_maximum_fusion, pred[6,128,384]{1,2,0:T(8,128)(4,1)S(1)} %fusion.13), kind=kOutput, calls=%fused_computation.25 | convolution fusion | flops 157089792 | bytes 6021120 | tf_op jit(solution)/shard_map/nhgqk,nkhd->nqhgd/dot_general | solution.py:119
  192.9 1.2 slice-done.2
  195.0 4.5 %add_convert_fusion = bf16[768,4096]{1,0:T(8,128)(2,1)} fusion(f32[768,4096]{1,0:T(8,128)S(1)} %bitcast.100, bf16[384,4096]{1,0:T(8,128)(2,1)S(1)} %copy-done.2, bf16[32,8,6,128]{3,2,1,0:T(8,128)(2,1)S(1)} %bitcast.111), kind=kOutput, calls=%fused_computation.10 | convolution fusion | flops 1616904192 | bytes 21495808 | tf_op jit(solution)/shard_map/dot_general | solution.py:186
  199.6 47.5 %reduce-scatter.2.cloned.1.call-done = bf16[96,4096]{1,0:T(8,128)(2,1)} async-done(((bf16[768,4096]{1,0:T(8,128)(2,1)}), bf16[96,4096]{1,0:T(8,128)(2,1)}) %reduce-scatter.2.cloned.1.call-update) | async-done | bytes 786448 | tf_op jit(solution)/shard_map/reduce_scatter | solution.py:183
  (104 shorter events, 12.6 us)
Async XLA Ops:
  6.5 51.6 %copy-start.7 = (bf16[768,512]{1,0:T(8,128)(2,1)S(1)}, bf16[768,512]{1,0:T(8,128)(2,1)}, u32[]{:S(2)}) copy-start(bf16[768,512]{1,0:T(8,128)(2,1)} %param.11) | copy-start | bytes 2359300
  6.5 107.9 %all-gather.3.cloned.1.call-start = ((), (), s32[]{:S(2)}) async-start(), calls=%async_computation.1 | async-start | bytes 5406720 | tf_op jit(solution)/shard_map/all_gather | solution.py:57
  8.2 165.4 %all-gather.5.cloned.1.call-start = ((), (), s32[]{:S(2)}) async-start(), calls=%async_computation.2 | async-start | bytes 3244032 | tf_op jit(solution)/shard_map/all_gather | solution.py:57
  8.3 11.9 %collective-permute-start = (bf16[768,512]{1,0:T(8,128)(2,1)}, bf16[768,512]{1,0:T(8,128)(2,1)S(1)}, u32[]{:S(2)}, u32[]{:S(2)}) collective-permute-start(bf16[768,512]{1,0:T(8,128)(2,1)} %param.11), channel_id=1, source_target_pairs={{0,1},{1,2},{2,3},{3,4},{4,5},{5,6},{6,7},{7,0},{8,9},{9,10},{10,1... | collective-permute-start | bytes 2359304 | tf_op jit(solution)/shard_map/ppermute | solution.py:29
  20.2 11.3 %collective-permute-start.1 = (bf16[768,512]{1,0:T(8,128)(2,1)S(1)}, bf16[768,512]{1,0:T(8,128)(2,1)S(1)}, u32[]{:S(2)}, u32[]{:S(2)}) collective-permute-start(bf16[768,512]{1,0:T(8,128)(2,1)S(1)} %collective-permute-done), channel_id=1, source_target_pairs={{0,1},{1,2},{2,3},{3,4},{4,5},{5,6},{6,7},{7,0},{8,9},{9,10},{10,1... | collective-permute-start | bytes 2359304 | tf_op jit(solution)/shard_map/ppermute | solution.py:29
  22.6 12.8 %collective-permute-start.4 = (bf16[768,512]{1,0:T(8,128)(2,1)}, bf16[768,512]{1,0:T(8,128)(2,1)S(1)}, u32[]{:S(2)}, u32[]{:S(2)}) collective-permute-start(bf16[768,512]{1,0:T(8,128)(2,1)} %param.11), channel_id=1, source_target_pairs={{1,0},{2,1},{3,2},{4,3},{5,4},{6,5},{7,6},{0,7},{9,8},{10,9},{11,1... | collective-permute-start | bytes 2359304 | tf_op jit(solution)/shard_map/ppermute | solution.py:31
  25.8 221.2 %reduce-scatter.2.cloned.1.call-start = ((), (), s32[]{:S(2)}) async-start(), calls=%async_computation.3 | async-start | bytes 7077888 | tf_op jit(solution)/shard_map/reduce_scatter | solution.py:183
  31.5 11.4 %collective-permute-start.2 = (bf16[768,512]{1,0:T(8,128)(2,1)S(1)}, bf16[768,512]{1,0:T(8,128)(2,1)S(1)}, u32[]{:S(2)}, u32[]{:S(2)}) collective-permute-start(bf16[768,512]{1,0:T(8,128)(2,1)S(1)} %collective-permute-done.1), channel_id=1, source_target_pairs={{0,1},{1,2},{2,3},{3,4},{4,5},{5,6},{6,7},{7,0},{8,9},{9,10},{10,1... | collective-permute-start | bytes 2359304 | tf_op jit(solution)/shard_map/ppermute | solution.py:29
  35.3 11.8 %collective-permute-start.5 = (bf16[768,512]{1,0:T(8,128)(2,1)S(1)}, bf16[768,512]{1,0:T(8,128)(2,1)S(1)}, u32[]{:S(2)}, u32[]{:S(2)}) collective-permute-start(bf16[768,512]{1,0:T(8,128)(2,1)S(1)} %collective-permute-done.4), channel_id=1, source_target_pairs={{1,0},{2,1},{3,2},{4,3},{5,4},{6,5},{7,6},{0,7},{9,8},{10,9},{11,1... | collective-permute-start | bytes 2359304 | tf_op jit(solution)/shard_map/ppermute | solution.py:31
  42.9 11.4 %collective-permute-start.3 = (bf16[768,512]{1,0:T(8,128)(2,1)S(1)}, bf16[768,512]{1,0:T(8,128)(2,1)S(1)}, u32[]{:S(2)}, u32[]{:S(2)}) collective-permute-start(bf16[768,512]{1,0:T(8,128)(2,1)S(1)} %collective-permute-done.2), channel_id=1, source_target_pairs={{0,1},{1,2},{2,3},{3,4},{4,5},{5,6},{6,7},{7,0},{8,9},{9,10},{10,1... | collective-permute-start | bytes 2359304 | tf_op jit(solution)/shard_map/ppermute | solution.py:29
  47.2 13.8 %collective-permute-start.6 = (bf16[768,512]{1,0:T(8,128)(2,1)S(1)}, bf16[768,512]{1,0:T(8,128)(2,1)S(1)}, u32[]{:S(2)}, u32[]{:S(2)}) collective-permute-start(bf16[768,512]{1,0:T(8,128)(2,1)S(1)} %collective-permute-done.5), channel_id=1, source_target_pairs={{1,0},{2,1},{3,2},{4,3},{5,4},{6,5},{7,6},{0,7},{9,8},{10,9},{11,1... | collective-permute-start | bytes 2359304 | tf_op jit(solution)/shard_map/ppermute | solution.py:31
  68.6 4.8 %copy-start = (bf16[8,768,512]{2,1,0:T(8,128)(2,1)S(1)}, bf16[8,768,512]{2,1,0:T(8,128)(2,1)}, u32[]{:S(2)}) copy-start(bf16[8,768,512]{2,1,0:T(8,128)(2,1)} %gather_fusion) | copy-start | bytes 18874372
  93.0 12.7 %copy-start.12 = (f32[4096]{0:T(1024)S(1)}, f32[4096]{0:T(1024)}, u32[]{:S(2)}) copy-start(f32[4096]{0:T(1024)} %param.12) | copy-start | bytes 49156
  119.2 12.5 %slice-start.3 = ((s8[6291456]{0:T(1024)(128)(4,1)}), s8[2097152]{0:T(1024)(128)(4,1)S(1)}, s32[]{:S(2)}) async-start(s8[6291456]{0:T(1024)(128)(4,1)} %bitcast.101), calls=%async_computation.7 | async-start | bytes 4194304
  122.0 9.7 %slice-start.4 = ((s8[6291456]{0:T(1024)(128)(4,1)}), s8[4194304]{0:T(1024)(128)(4,1)S(1)}, s32[]{:S(2)}) async-start(s8[6291456]{0:T(1024)(128)(4,1)} %bitcast.101), calls=%async_computation.8 | async-start | bytes 8388608
  122.0 9.7 %copy-start.6 = (bf16[128,4096]{1,0:T(8,128)(2,1)S(1)}, bf16[128,4096]{1,0:T(8,128)(2,1)}, u32[]{:S(2)}) copy-start(bf16[128,4096]{1,0:T(8,128)(2,1)} %copy.63) | copy-start | bytes 3145732
  122.0 10.8 %copy-start.3 = (bf16[256,4096]{1,0:T(8,128)(2,1)S(1)}, bf16[256,4096]{1,0:T(8,128)(2,1)}, u32[]{:S(2)}) copy-start(bf16[256,4096]{1,0:T(8,128)(2,1)} %copy.70) | copy-start | bytes 6291460
  127.1 4.6 %copy-start.10 = (bf16[768,128]{1,0:T(8,128)(2,1)}, bf16[768,128]{1,0:T(8,128)(2,1)S(1)}, u32[]{:S(2)}) copy-start(bf16[768,128]{1,0:T(8,128)(2,1)S(1)} %convolution_convert_fusion.1) | copy-start | bytes 589828
  127.1 18.8 %collective-permute-start.7 = (bf16[8,128]{1,0:T(8,128)(2,1)S(1)}, bf16[8,128]{1,0:T(8,128)(2,1)S(1)}, u32[]{:S(2)}, u32[]{:S(2)}) collective-permute-start(bf16[8,128]{1,0:T(8,128)(2,1)S(1)} %get-tuple-element.22), channel_id=1, source_target_pairs={{0,8},{8,16},{16,24},{24,32},{32,40},{40,48},{48,56},{56,64},{64,7... | collective-permute-start | bytes 6152 | tf_op jit(solution)/shard_map/ppermute | solution.py:43
  130.2 15.7 %collective-permute-start.8 = (bf16[8,128]{1,0:T(8,128)(2,1)S(1)}, bf16[8,128]{1,0:T(8,128)(2,1)S(1)}, u32[]{:S(2)}, u32[]{:S(2)}) collective-permute-start(bf16[8,128]{1,0:T(8,128)(2,1)S(1)} %get-tuple-element.23), channel_id=1, source_target_pairs={{8,0},{16,8},{24,16},{32,24},{40,32},{48,40},{56,48},{64,56},{72,6... | collective-permute-start | bytes 6152 | tf_op jit(solution)/shard_map/ppermute | solution.py:46
  132.8 2.8 %slice-start.5 = ((s8[6291456]{0:T(1024)(128)(4,1)}), s8[4194304]{0:T(1024)(128)(4,1)S(1)}, s32[]{:S(2)}) async-start(s8[6291456]{0:T(1024)(128)(4,1)} %bitcast.105), calls=%async_computation.9 | async-start | bytes 8388608
  132.8 1.9 copy-start.13
  132.8 2.0 copy-start.14
  132.8 2.3 copy-start.4
  132.8 2.3 copy-start.5
  132.9 3.0 %slice-start.6 = ((s8[6291456]{0:T(1024)(128)(4,1)}), s8[2097152]{0:T(1024)(128)(4,1)S(1)}, s32[]{:S(2)}) async-start(s8[6291456]{0:T(1024)(128)(4,1)} %bitcast.105), calls=%async_computation.10 | async-start | bytes 4194304
  135.2 10.7 %copy-start.11 = (bf16[768,128]{1,0:T(8,128)(2,1)S(1)}, bf16[768,128]{1,0:T(8,128)(2,1)}, u32[]{:S(2)}) copy-start(bf16[768,128]{1,0:T(8,128)(2,1)} %copy-done.10) | copy-start | bytes 589828
  138.2 7.9 %copy-start.8 = (bf16[768,128]{0,1:T(8,128)(2,1)}, bf16[768,128]{0,1:T(8,128)(2,1)S(1)}, u32[]{:S(2)}) copy-start(bf16[768,128]{0,1:T(8,128)(2,1)S(1)} %convolution_convert_fusion) | copy-start | bytes 589828
  139.4 41.9 %collective-permute-start.10 = (bf16[128,256]{0,1:T(8,128)(2,1)}, bf16[128,256]{0,1:T(8,128)(2,1)}, u32[]{:S(2)}, u32[]{:S(2)}) collective-permute-start(bf16[128,256]{0,1:T(8,128)(2,1)} %get-tuple-element.17), channel_id=1, source_target_pairs={{8,0},{16,8},{24,16},{32,24},{40,32},{48,40},{56,48},{64,56},{72,6... | collective-permute-start | bytes 196616 | tf_op jit(solution)/shard_map/ppermute | solution.py:46
  140.7 40.6 %collective-permute-start.9 = (bf16[128,256]{0,1:T(8,128)(2,1)S(1)}, bf16[128,256]{0,1:T(8,128)(2,1)}, u32[]{:S(2)}, u32[]{:S(2)}) collective-permute-start(bf16[128,256]{0,1:T(8,128)(2,1)S(1)} %get-tuple-element.16), channel_id=1, source_target_pairs={{0,8},{8,16},{16,24},{24,32},{32,40},{40,48},{48,56},{56,64},{64,7... | collective-permute-start | bytes 196616 | tf_op jit(solution)/shard_map/ppermute | solution.py:43
  173.6 7.7 %copy-start.9 = (bf16[768,128]{0,1:T(8,128)(2,1)S(1)}, bf16[768,128]{0,1:T(8,128)(2,1)}, u32[]{:S(2)}) copy-start(bf16[768,128]{0,1:T(8,128)(2,1)} %copy-done.8) | copy-start | bytes 589828
  184.4 2.1 copy-start.1
  188.0 4.2 %slice-start = ((s8[12582912]{0:T(1024)(128)(4,1)}), s8[4194304]{0:T(1024)(128)(4,1)S(1)}, s32[]{:S(2)}) async-start(s8[12582912]{0:T(1024)(128)(4,1)} %bitcast.99), calls=%async_computation.4 | async-start | bytes 8388608
  188.0 4.9 %slice-start.1 = ((s8[12582912]{0:T(1024)(128)(4,1)}), s8[4194304]{0:T(1024)(128)(4,1)S(1)}, s32[]{:S(2)}) async-start(s8[12582912]{0:T(1024)(128)(4,1)} %bitcast.99), calls=%async_computation.5 | async-start | bytes 8388608
  188.0 6.1 %slice-start.2 = ((s8[12582912]{0:T(1024)(128)(4,1)}), s8[4194304]{0:T(1024)(128)(4,1)S(1)}, s32[]{:S(2)}) async-start(s8[12582912]{0:T(1024)(128)(4,1)} %bitcast.99), calls=%async_computation.6 | async-start | bytes 8388608
  188.0 7.0 %copy-start.2 = (bf16[384,4096]{1,0:T(8,128)(2,1)S(1)}, bf16[384,4096]{1,0:T(8,128)(2,1)}, u32[]{:S(2)}) copy-start(bf16[384,4096]{1,0:T(8,128)(2,1)} %all-gather.5.cloned.1.call-done) | copy-start | bytes 9437188
Sparse Core Ops, SparseCore 0:
  9.9 85.4 all-gather.2
  97.9 75.7 all-gather.4
  199.7 47.3 reduce-scatter.1
